TPU v7x, 32 devices: a whole 2x2x4 slice. The times are simulated.
32 devices in a mesh: fs: 8 (over z, core), tp: 4 (over y, x).
Axes of the slice: x: 2, y: 2, z: 4, core: 2. Of those that a mesh axis runs over, the one named last changes fastest.
Arguments:
- latent: bfloat16 [16384, 1024], P('fs'), may hold values from -6 to 6
- key_cotangent: bfloat16 [16384, 512], P('fs', 'tp'), may hold values from -0.046875 to 0.046875
- value_cotangent: bfloat16 [16384, 512], P('fs', 'tp'), may hold values from -0.046875 to 0.046875
- key_weight: float32 [1024, 512], P('fs', 'tp'), may hold values from -50 to 50
- value_weight: float32 [1024, 512], P('fs', 'tp'), may hold values from -50 to 50
- key_projector: bfloat16 [1024, 256], replicated, may hold values from -0.1875 to 0.1875
- value_projector: bfloat16 [1024, 256], replicated, may hold values from -0.1875 to 0.1875
- key_first: float32 [256, 512], P(None, 'tp'), may hold values from -6 to 6
- key_second: float32 [256, 512], P(None, 'tp'), may hold values from 0.3 to 3
- value_first: float32 [256, 512], P(None, 'tp'), may hold values from -6 to 6
- value_second: float32 [256, 512], P(None, 'tp'), may hold values from 0.3 to 3
Outputs:
- key_renewed: float32 [1024, 512], P('fs', 'tp')
- value_renewed: float32 [1024, 512], P('fs', 'tp')
- key_step: float32 [1024, 512], P('fs', 'tp')
- value_step: float32 [1024, 512], P('fs', 'tp')
- key_first_new: float32 [256, 512], P(None, 'tp')
- key_second_new: float32 [256, 512], P(None, 'tp')
- value_first_new: float32 [256, 512], P(None, 'tp')
- value_second_new: float32 [256, 512], P(None, 'tp')
- key_copy: bfloat16 [1024, 512], P(None, 'tp')
- value_copy: bfloat16 [1024, 512], P(None, 'tp')
All inputs are finite; a program needn't handle non-finite values.
Results may differ from a plain program's by a relative error of at most 0.015.
Values may be sent and summed in bfloat16 or wider, within the bound.
A program may use at most 64 MiB of HBM per device.

v0:
```python
import jax
import jax.numpy as jnp
from jax import lax
from jax.sharding import PartitionSpec as P

EPSILON = 1e-08
FIRST_DECAY = 0.7
SECOND_DECAY = 0.8
LEARN_RATE = 0.2


def contract_rows(left, right):
    return jnp.dot(left.T, right, precision=lax.Precision.HIGHEST)


def moments_and_step(
    weight, factor_rows, projected, first_moment, second, total_squares, entry_count
):
    first_new = FIRST_DECAY * first_moment + (1.0 - FIRST_DECAY) * projected
    second_new = SECOND_DECAY * second + (1.0 - SECOND_DECAY) * projected * projected
    normalized = first_new / (jnp.sqrt(second_new) + EPSILON)
    direction = jnp.dot(
        factor_rows.astype(jnp.float32), normalized, precision=lax.Precision.HIGHEST
    )
    step_scale = LEARN_RATE * jnp.sqrt(total_squares / entry_count)
    weight_step = step_scale * direction
    return (weight - weight_step, weight_step, first_new, second_new)


def body(
    latent,
    key_cotangent,
    value_cotangent,
    key_weight,
    value_weight,
    key_projector,
    value_projector,
    key_first,
    key_second,
    value_first,
    value_second,
):
    row_count = key_weight.shape[0]
    row_start = lax.axis_index("fs") * row_count
    key_rows = lax.dynamic_slice_in_dim(key_projector, row_start, row_count, 0)
    value_rows = lax.dynamic_slice_in_dim(value_projector, row_start, row_count, 0)
    key_squares, value_squares = lax.psum(
        (jnp.sum(key_weight * key_weight), jnp.sum(value_weight * value_weight)), ("fs", "tp")
    )
    devices = lax.axis_size("fs") * lax.axis_size("tp")
    key_entries = float(key_weight.size * devices)
    value_entries = float(value_weight.size * devices)
    rank = key_projector.shape[1]
    factors = jnp.concatenate([key_projector, value_projector], axis=1)
    reduced = jnp.dot(latent, factors, preferred_element_type=jnp.float32)
    key_term = contract_rows(reduced[:, :rank], key_cotangent.astype(jnp.float32))
    value_term = contract_rows(reduced[:, rank:], value_cotangent.astype(jnp.float32))
    key_projected, value_projected = (
        lax.psum(key_term.astype(jnp.bfloat16), "fs").astype(jnp.float32),
        lax.psum(value_term.astype(jnp.bfloat16), "fs").astype(jnp.float32),
    )
    key_renewed, key_step, key_first_new, key_second_new = moments_and_step(
        key_weight, key_rows, key_projected, key_first, key_second, key_squares, key_entries
    )
    value_renewed, value_step, value_first_new, value_second_new = moments_and_step(
        value_weight,
        value_rows,
        value_projected,
        value_first,
        value_second,
        value_squares,
        value_entries,
    )
    key_copy, value_copy = (
        lax.all_gather(key_renewed.astype(jnp.bfloat16), "fs", axis=0, tiled=True),
        lax.all_gather(value_renewed.astype(jnp.bfloat16), "fs", axis=0, tiled=True),
    )
    return (
        key_renewed,
        value_renewed,
        key_step,
        value_step,
        key_first_new,
        key_second_new,
        value_first_new,
        value_second_new,
        key_copy,
        value_copy,
    )


def solution(mesh):
    return jax.shard_map(
        body,
        mesh=mesh,
        in_specs=(
            P("fs", None),
            P("fs", "tp"),
            P("fs", "tp"),
            P("fs", "tp"),
            P("fs", "tp"),
            P(),
            P(),
            P(None, "tp"),
            P(None, "tp"),
            P(None, "tp"),
            P(None, "tp"),
        ),
        out_specs=(
            P("fs", "tp"),
            P("fs", "tp"),
            P("fs", "tp"),
            P("fs", "tp"),
            P(None, "tp"),
            P(None, "tp"),
            P(None, "tp"),
            P(None, "tp"),
            P(None, "tp"),
            P(None, "tp"),
        ),
        check_vma=False,
    )
```

profile of v0, /device:TPU:0, one launch (start us, length us, event | category | flops | bytes accessed | tf_op | source)
XLA Modules:
  0.0 116.0 jit_solution(1919215381122965088)
XLA Ops:
  7.2 0.0 copy-start
  7.2 0.0 copy-start.1
  7.2 0.0 all-reduce.4.cloned.1.call-start
  7.2 5.0 %convolution_bitcast_fusion = f32[2048,512]{0,1:T(8,128)S(1)} fusion(bf16[2048,1024]{1,0:T(8,128)(2,1)} %param.11, bf16[1024,256]{1,0:T(8,128)(2,1)} %param.17, bf16[1024,256]{1,0:T(8,128)(2,1)} %param.16), kind=kOutput, calls=%fused_computation | convolution fusion | flops 2149580800 | bytes 9437184 | tf_op jit(solution)/shard_map/dot_general | solution.py:55
  12.2 0.0 copy-done
  12.2 0.0 copy-start.10
  12.2 0.0 copy-start.11
  12.3 0.0 copy-start.2
  12.3 0.0 copy-start.3
  12.3 0.0 copy-start.4
  12.3 0.0 copy-start.5
  12.3 1.7 %fusion.4 = bf16[256,128]{1,0:T(8,128)(2,1)} fusion(bf16[2048,128]{1,0:T(8,128)(2,1)S(1)} %copy-done, f32[2048,512]{0,1:T(8,128)S(1)} %convolution_bitcast_fusion), kind=kOutput, calls=%fused_computation.5 | convolution fusion | flops 805339136 | bytes 2686976 | tf_op jit(solution)/shard_map/dot_general | solution.py:13
  14.0 0.0 copy-done.1
  14.0 1.7 %fusion.7 = bf16[256,128]{1,0:T(8,128)(2,1)} fusion(bf16[2048,128]{1,0:T(8,128)(2,1)S(1)} %copy-done.1, f32[2048,512]{0,1:T(8,128)S(1)} %convolution_bitcast_fusion), kind=kOutput, calls=%fused_computation.6 | convolution fusion | flops 805339136 | bytes 2686976 | tf_op jit(solution)/shard_map/dot_general | solution.py:13
  15.7 0.0 all-reduce.4.cloned.1.call-update
  15.7 0.6 multiply_reduce_fusion
  16.4 42.3 %all-reduce = (f32[]{:T(128)}, f32[]{:T(128)}) all-reduce(f32[]{:T(128)} %get-tuple-element.25, f32[]{:T(128)} %get-tuple-element.24), channel_id=1, replica_groups=mesh['fs'=8,'tp'=4] {'fs','tp'}, use_global_device_ids=true, to_apply=%region_1.0 | all-reduce | flops 2 | bytes 16 | tf_op jit(solution)/shard_map/psum | solution.py:47
  60.0 13.8 %all-reduce.4.cloned.1.call-done = (bf16[256,128]{1,0:T(8,128)(2,1)}, bf16[256,128]{1,0:T(8,128)(2,1)}) async-done(((bf16[256,128]{1,0:T(8,128)(2,1)}, bf16[256,128]{1,0:T(8,128)(2,1)}), (bf16[256,128]{1,0:T(8,128)(2,1)}, bf16[256,128]{1,0:T(8,128)(2,1)})) %all-reduce.4.cloned.1.call-update) | async-done | bytes 131088 | tf_op jit(solution)/shard_map/psum | solution.py:59
  73.8 0.0 copy-done.2
  73.8 0.9 fusion.15
  74.7 0.0 copy-start.6
  74.7 0.0 copy-start.7
  74.7 1.9 %fusion.33 = (bf16[128,128]{1,0:T(8,128)(2,1)S(1)}, f32[128,128]{1,0:T(8,128)}, f32[128,128]{1,0:T(8,128)}) fusion(f32[128,128]{1,0:T(8,128)S(1)} %copy-done.10, f32[256,128]{1,0:T(8,128)S(1)} %get-tuple-element.40, f32[256,128]{1,0:T(8,128)S(1)} %get-tuple-element.41, bf16[1024,256]{1,0:T(8,128)(2,1)} %param.16, s32[]{:T(128)S(6)} %select_n.4, f32[]{:T(128)S(6)} %mul.58), kind=kOutput, calls=%fused_computation.38 | convolution fusion | flops 50446336 | bytes 557064 | tf_op jit(solution)/shard_map/dot_general | solution.py:22
  76.6 14.2 %all_gather.6 = bf16[1024,128]{1,0:T(8,128)(2,1)S(1)} all-gather(bf16[128,128]{1,0:T(8,128)(2,1)S(1)} %get-tuple-element.16), channel_id=1, replica_groups=mesh['fs'=8,'tp'=4] {'fs'}, dimensions={0}, use_global_device_ids=true | all-gather | bytes 294912 | tf_op jit(solution)/shard_map/all_gather | solution.py:75
  90.7 0.9 fusion.16
  91.6 0.0 copy-start.8
  91.6 0.0 copy-start.9
  91.6 1.9 %fusion.32 = (bf16[128,128]{1,0:T(8,128)(2,1)S(1)}, f32[128,128]{1,0:T(8,128)}, f32[128,128]{1,0:T(8,128)}) fusion(f32[128,128]{1,0:T(8,128)S(1)} %copy-done.11, f32[256,128]{1,0:T(8,128)S(1)} %get-tuple-element.42, f32[256,128]{1,0:T(8,128)S(1)} %get-tuple-element.43, bf16[1024,256]{1,0:T(8,128)(2,1)} %param.17, s32[]{:T(128)S(6)} %select_n.4, f32[]{:T(128)S(6)} %mul.68), kind=kOutput, calls=%fused_computation.37 | convolution fusion | flops 50446336 | bytes 557064 | tf_op jit(solution)/shard_map/dot_general | solution.py:22
  93.5 14.2 %all_gather.7 = bf16[1024,128]{1,0:T(8,128)(2,1)S(1)} all-gather(bf16[128,128]{1,0:T(8,128)(2,1)S(1)} %get-tuple-element.14), channel_id=1, replica_groups=mesh['fs'=8,'tp'=4] {'fs'}, dimensions={0}, use_global_device_ids=true | all-gather | bytes 294912 | tf_op jit(solution)/shard_map/all_gather | solution.py:76
  107.7 0.7 copy.25
  108.4 0.7 copy.26
  109.1 0.0 copy-done.7
  (8 shorter events, 0.0 us)
Async XLA Ops:
  7.2 5.0 %copy-start = (bf16[2048,128]{1,0:T(8,128)(2,1)S(1)}, bf16[2048,128]{1,0:T(8,128)(2,1)}, u32[]{:S(2)}) copy-start(bf16[2048,128]{1,0:T(8,128)(2,1)} %param.12) | copy-start | bytes 1572868
  7.2 6.8 %copy-start.1 = (bf16[2048,128]{1,0:T(8,128)(2,1)S(1)}, bf16[2048,128]{1,0:T(8,128)(2,1)}, u32[]{:S(2)}) copy-start(bf16[2048,128]{1,0:T(8,128)(2,1)} %param.13) | copy-start | bytes 1572868
  7.2 66.6 %all-reduce.4.cloned.1.call-start = ((), (), s32[]{:S(2)}) async-start(), calls=%async_computation | async-start | bytes 262144 | tf_op jit(solution)/shard_map/psum | solution.py:59
  12.2 3.5 %copy-start.10 = (f32[128,128]{1,0:T(8,128)S(1)}, f32[128,128]{1,0:T(8,128)}, u32[]{:S(2)}) copy-start(f32[128,128]{1,0:T(8,128)} %param.14) | copy-start | bytes 196612
  12.2 3.5 %copy-start.11 = (f32[128,128]{1,0:T(8,128)S(1)}, f32[128,128]{1,0:T(8,128)}, u32[]{:S(2)}) copy-start(f32[128,128]{1,0:T(8,128)} %param.15) | copy-start | bytes 196612
  12.3 61.5 %copy-start.2 = (f32[256,128]{1,0:T(8,128)S(1)}, f32[256,128]{1,0:T(8,128)}, u32[]{:S(2)}) copy-start(f32[256,128]{1,0:T(8,128)} %param.19) | copy-start | bytes 393220
  12.3 61.5 %copy-start.3 = (f32[256,128]{1,0:T(8,128)S(1)}, f32[256,128]{1,0:T(8,128)}, u32[]{:S(2)}) copy-start(f32[256,128]{1,0:T(8,128)} %param.18) | copy-start | bytes 393220
  12.3 78.5 %copy-start.4 = (f32[256,128]{1,0:T(8,128)S(1)}, f32[256,128]{1,0:T(8,128)}, u32[]{:S(2)}) copy-start(f32[256,128]{1,0:T(8,128)} %param.21) | copy-start | bytes 393220
  12.3 78.4 %copy-start.5 = (f32[256,128]{1,0:T(8,128)S(1)}, f32[256,128]{1,0:T(8,128)}, u32[]{:S(2)}) copy-start(f32[256,128]{1,0:T(8,128)} %param.20) | copy-start | bytes 393220
  74.7 34.5 %copy-start.6 = (f32[256,128]{1,0:T(8,128)}, f32[256,128]{1,0:T(8,128)S(1)}, u32[]{:S(2)}) copy-start(f32[256,128]{1,0:T(8,128)S(1)} %get-tuple-element.41) | copy-start | bytes 393220
  74.7 34.4 %copy-start.7 = (f32[256,128]{1,0:T(8,128)}, f32[256,128]{1,0:T(8,128)S(1)}, u32[]{:S(2)}) copy-start(f32[256,128]{1,0:T(8,128)S(1)} %get-tuple-element.40) | copy-start | bytes 393220
  91.6 17.5 %copy-start.8 = (f32[256,128]{1,0:T(8,128)}, f32[256,128]{1,0:T(8,128)S(1)}, u32[]{:S(2)}) copy-start(f32[256,128]{1,0:T(8,128)S(1)} %get-tuple-element.43) | copy-start | bytes 393220
  91.6 17.5 %copy-start.9 = (f32[256,128]{1,0:T(8,128)}, f32[256,128]{1,0:T(8,128)S(1)}, u32[]{:S(2)}) copy-start(f32[256,128]{1,0:T(8,128)S(1)} %get-tuple-element.42) | copy-start | bytes 393220
Sparse Core Ops, SparseCore 0:
  15.8 57.8 all-reduce.3
where the time goes:
time: 116 us
  blocking collectives  70.7 us (61%)
  between operations  15.6 us (13%)
  waiting for transfers between devices  13.8 us (12%)
  matrix products  12.1 us (10%)
  other arithmetic  2.38 us (2%)
  local copies, waits for them, and re-layouts  1.48 us (1%)
    psum x1, blocking collectives, body(): lax.psum((jnp.sum(key_weight * key_weight), jnp.sum(value_weight * value_...  42.3 us
    all_gather x1, blocking collectives, body(): lax.all_gather(value_renewed.astype(jnp.bfloat16), 'fs', axis=0, tiled=True)  14.2 us
    all_gather x1, blocking collectives, body(): lax.all_gather(key_renewed.astype(jnp.bfloat16), 'fs', axis=0, tiled=True)  14.2 us
    psum x1, waiting for transfers between devices, body(): lax.psum(key_term.astype(jnp.bfloat16), 'fs').astype(jnp.float32)  13.8 us
    dot_general x1, matrix products, body(): reduced = jnp.dot(latent, factors, preferred_element_type=jnp.float32)  4.96 us
    dot_general x2, matrix products, moments_and_step(): jnp.dot(factor_rows.astype(jnp.float32), normalized, precision=lax.Precis...  3.7 us
    dot_general x2, matrix products, contract_rows(): return jnp.dot(left.T, right, precision=lax.Precision.HIGHEST)  3.39 us
  transfers between devices with their start and end apart: 1, of which 1 were waited for; matrix products, arithmetic and copies ran while one was open for 1% of the time, Pallas kernels for 0%

commit v1 on v0

v1 whole, which is shorter than its diff:
```python
import functools

import jax
import jax.numpy as jnp
from jax import lax
from jax.experimental import pallas as pl
from jax.experimental.pallas import tpu as pltpu
from jax.sharding import PartitionSpec as P

EPSILON = 1e-08
FIRST_DECAY = 0.7
SECOND_DECAY = 0.8
LEARN_RATE = 0.2
CHUNKS = 4
MESH = pl.DeviceIdType.MESH
HBM = pl.BlockSpec(memory_space=pltpu.MemorySpace.HBM)
VMEM = pl.BlockSpec(memory_space=pltpu.MemorySpace.VMEM)


def exchange_kernel(
    n,
    m,
    latent,
    key_cot,
    value_cot,
    key_weight,
    value_weight,
    key_proj,
    value_proj,
    gathered,
    weights,
    squares,
    latent_v,
    cot_v,
    cot_t,
    weight_v,
    proj_v,
    partial,
    received,
    tp_squares,
    load_sem,
    latent_sem,
    rs_send,
    rs_recv,
    ag_send,
    ag_recv,
    w_send,
    w_recv,
    f_send,
    f_recv,
    t_send,
    t_recv,
    s_send,
    s_recv,
):
    me = lax.axis_index("fs")
    mine = lax.axis_index("tp")
    core = lax.rem(me, 2)
    partner = me + 1 - 2 * core
    half = n // 2
    tokens, width = latent.shape
    step = width // CHUNKS
    rank = key_proj.shape[1]
    cols = key_cot.shape[1]
    piece = partial.shape[0] // n
    f32, bf16 = jnp.float32, jnp.bfloat16

    loads = [
        pltpu.make_async_copy(src, dst, load_sem.at[i])
        for i, (src, dst) in enumerate(
            (
                (key_weight, weight_v.at[0]),
                (value_weight, weight_v.at[1]),
                (key_cot, cot_v.at[0]),
                (value_cot, cot_v.at[1]),
                (key_proj, proj_v.at[0]),
                (value_proj, proj_v.at[1]),
            )
        )
    ]
    streams = [
        pltpu.make_async_copy(
            latent.at[:, pl.ds(c * step, step)], latent_v.at[c], latent_sem.at[c]
        )
        for c in range(CHUNKS)
    ]
    for copy in loads[:4]:
        copy.start()
    streams[0].start()
    for copy in loads[4:]:
        copy.start()
    for copy in streams[1:]:
        copy.start()

    barrier = pltpu.get_barrier_semaphore()
    for d in range(1, n):
        pl.semaphore_signal(
            barrier, inc=1, device_id={"fs": lax.rem(me + d, n)}, device_id_type=MESH
        )
    for d in range(1, m):
        pl.semaphore_signal(
            barrier, inc=1, device_id={"tp": lax.rem(mine + d, m)}, device_id_type=MESH
        )

    def send(src, dst, send_sem, recv_sem, where):
        copy = pltpu.make_async_remote_copy(
            src_ref=src,
            dst_ref=dst,
            send_sem=send_sem,
            recv_sem=recv_sem,
            device_id=where,
            device_id_type=MESH,
        )
        copy.start()
        return copy

    def arrived(ref, sem):
        pltpu.make_async_remote_copy(
            src_ref=ref,
            dst_ref=ref,
            send_sem=sem,
            recv_sem=sem,
            device_id={"fs": partner},
            device_id_type=MESH,
        ).wait_recv()

    sent = []
    loads[0].wait()
    loads[1].wait()
    for i in range(2):
        w = weight_v[i]
        weights[me, i] = w.astype(bf16)
        tp_squares[mine, pl.ds(8 * i, 8), :] = jnp.sum(
            (w * w).reshape(w.shape[0] // 8, 8, w.shape[1]), axis=0
        )
    loads[2].wait()
    loads[3].wait()
    for i in range(2):
        cot_t[pl.ds(i * cols, cols), :] = cot_v[i].T

    pl.semaphore_wait(barrier, n - 1 + m - 1)

    def send_weights(d):
        sent.append(
            send(
                weights.at[me],
                weights.at[me],
                w_send.at[d],
                w_recv.at[me],
                {"fs": lax.rem(me + 2 * d, n)},
            )
        )

    for d in range(1, m):
        sent.append(
            send(
                tp_squares.at[mine],
                tp_squares.at[mine],
                t_send.at[d],
                t_recv.at[mine],
                {"tp": lax.rem(mine + d, m)},
            )
        )
    sent.append(
        send(
            weights.at[me], weights.at[me], f_send.at[0], f_recv.at[me], {"fs": partner}
        )
    )
    for d in range(1, half):
        send_weights(d)

    totals = [None, None]
    for c in range(CHUNKS):
        streams[c].wait()
        g = jnp.dot(cot_t[...], latent_v[c], preferred_element_type=f32).astype(bf16)
        if c == 0:
            loads[4].wait()
            loads[5].wait()
        for i in range(2):
            term = jnp.dot(
                g[i * cols : (i + 1) * cols],
                proj_v[i, pl.ds(c * step, step), :],
                preferred_element_type=f32,
            )
            totals[i] = term if totals[i] is None else totals[i] + term
    for i in range(2):
        partial[pl.ds(i * rank, rank), :] = totals[i].T.astype(bf16)

    for d in range(1, m):
        arrived(tp_squares.at[lax.rem(mine + d, m)], t_recv.at[lax.rem(mine + d, m)])
    squares[me] = jnp.sum(tp_squares[...], axis=0)

    for d in range(n - 1, 0, -1):
        peer = lax.rem(me + d, n)
        sent.append(
            send(
                partial.at[pl.ds(peer * piece, piece)],
                received.at[me],
                rs_send.at[d],
                rs_recv.at[me],
                {"fs": peer},
            )
        )
    received[me] = partial[pl.ds(pl.multiple_of(me * piece, piece), piece), :]
    for d in range(1, n):
        sent.append(
            send(
                squares.at[me],
                squares.at[me],
                s_send.at[d],
                s_recv.at[me],
                {"fs": lax.rem(me + d, n)},
            )
        )
    for d in range(1, n):
        peer = lax.rem(me + d, n)
        arrived(received.at[peer], rs_recv.at[peer])
    gathered[me] = jnp.sum(received[...].astype(f32), axis=0).astype(bf16)
    for d in range(n - 1, 0, -1):
        sent.append(
            send(
                gathered.at[me],
                gathered.at[me],
                ag_send.at[d],
                ag_recv.at[me],
                {"fs": lax.rem(me + d, n)},
            )
        )
    for d in range(1, half):
        source = lax.rem(me + 2 * d, n)
        arrived(weights.at[source], w_recv.at[source])
        sent.append(
            send(
                weights.at[source],
                weights.at[source],
                f_send.at[d],
                f_recv.at[source],
                {"fs": partner},
            )
        )
    for d in range(half):
        source = lax.rem(partner + 2 * d, n)
        arrived(weights.at[source], f_recv.at[source])
    for d in range(1, n):
        peer = lax.rem(me + d, n)
        arrived(squares.at[peer], s_recv.at[peer])
    for d in range(1, n):
        peer = lax.rem(me + d, n)
        arrived(gathered.at[peer], ag_recv.at[peer])
    for copy in sent:
        copy.wait_send()


def update_kernel(n, entries, *refs):
    (
        gathered,
        weights,
        squares,
        key_weight,
        value_weight,
        key_proj,
        value_proj,
        key_first,
        key_second,
        value_first,
        value_second,
    ) = refs[:11]
    outs = refs[11:]
    me = lax.axis_index("fs")
    f32, bf16 = jnp.float32, jnp.bfloat16
    parts = n // 2
    tile = jnp.sum(squares[...], axis=0)
    for i, (weight, proj, first, second) in enumerate(
        (
            (key_weight, key_proj, key_first, key_second),
            (value_weight, value_proj, value_first, value_second),
        )
    ):
        rows = weight.shape[0]
        rank, cols = first.shape
        projected = (
            gathered[i * parts : (i + 1) * parts].astype(f32).reshape(rank, cols)
        )
        first_new = FIRST_DECAY * first[...] + (1.0 - FIRST_DECAY) * projected
        second_new = (
            SECOND_DECAY * second[...] + (1.0 - SECOND_DECAY) * projected * projected
        )
        outs[4 + 2 * i][...] = first_new
        outs[5 + 2 * i][...] = second_new
        normalized = (first_new / (jnp.sqrt(second_new) + EPSILON)).astype(bf16)
        total = jnp.sum(tile[8 * i : 8 * i + 8], keepdims=True)
        scale = LEARN_RATE * jnp.sqrt(total / entries)
        own = proj[pl.ds(pl.multiple_of(me * rows, rows), rows), :]
        own_step = scale * jnp.dot(own, normalized, preferred_element_type=f32)
        outs[2 + i][...] = own_step
        outs[i][...] = weight[...] - own_step
        every = scale * jnp.dot(proj[...], normalized, preferred_element_type=f32)
        held = weights[:, i].astype(f32).reshape(n * rows, cols)
        outs[8 + i][...] = (held - every).astype(bf16)


def solution(mesh):
    n, m = mesh.shape["fs"], mesh.shape["tp"]

    def body(
        latent,
        key_cot,
        value_cot,
        key_weight,
        value_weight,
        key_proj,
        value_proj,
        key_first,
        key_second,
        value_first,
        value_second,
    ):
        f32, bf16 = jnp.float32, jnp.bfloat16
        sds = jax.ShapeDtypeStruct
        tokens, width = latent.shape
        rows, cols = key_weight.shape
        rank = key_proj.shape[1]
        piece = 2 * rank // n
        dma = pltpu.SemaphoreType.DMA
        gathered, weights, squares = pl.pallas_call(
            functools.partial(exchange_kernel, n, m),
            out_shape=(
                sds((n, piece, cols), bf16),
                sds((n, 2, rows, cols), bf16),
                sds((n, 16, cols), f32),
            ),
            in_specs=[HBM] * 7,
            out_specs=(VMEM,) * 3,
            scratch_shapes=[
                pltpu.VMEM((CHUNKS, tokens, width // CHUNKS), bf16),
                pltpu.VMEM((2, tokens, cols), bf16),
                pltpu.VMEM((2 * cols, tokens), bf16),
                pltpu.VMEM((2, rows, cols), f32),
                pltpu.VMEM((2, width, rank), bf16),
                pltpu.VMEM((2 * rank, cols), bf16),
                pltpu.VMEM((n, piece, cols), bf16),
                pltpu.VMEM((m, 16, cols), f32),
                dma((6,)),
                dma((CHUNKS,)),
                dma((n,)),
                dma((n,)),
                dma((n,)),
                dma((n,)),
                dma((n,)),
                dma((n,)),
                dma((n,)),
                dma((n,)),
                dma((m,)),
                dma((m,)),
                dma((n,)),
                dma((n,)),
            ],
            compiler_params=pltpu.CompilerParams(
                collective_id=0, has_side_effects=True, vmem_limit_bytes=24 << 20
            ),
        )(latent, key_cot, value_cot, key_weight, value_weight, key_proj, value_proj)
        small = sds((rows, cols), f32)
        moment = sds((rank, cols), f32)
        copy = sds((n * rows, cols), bf16)
        return pl.pallas_call(
            functools.partial(update_kernel, n, float(rows * cols * n * m)),
            out_shape=(small,) * 4 + (moment,) * 4 + (copy,) * 2,
            in_specs=[VMEM] * 11,
            out_specs=(VMEM,) * 10,
            compiler_params=pltpu.CompilerParams(vmem_limit_bytes=24 << 20),
        )(
            gathered,
            weights,
            squares,
            key_weight,
            value_weight,
            key_proj,
            value_proj,
            key_first,
            key_second,
            value_first,
            value_second,
        )

    split, column = P("fs", "tp"), P(None, "tp")
    return jax.shard_map(
        body,
        mesh=mesh,
        in_specs=(P("fs", None),) + (split,) * 4 + (P(),) * 2 + (column,) * 4,
        out_specs=(split,) * 4 + (column,) * 6,
        check_vma=False,
    )
```

time: 116 us -> 33.4 us (0.29)
  blocking collectives: 70.7 us -> 0 us
  Pallas kernels: 0 us -> 24.2 us
  between operations: 15.6 us -> 0.71 us
  waiting for transfers between devices: 13.8 us -> 0 us
  matrix products: 12.1 us -> 0 us
  local copies, waits for them, and re-layouts: 1.48 us -> 8.04 us
  other arithmetic: 2.38 us -> 0 us
    psum x1 -> x0, blocking collectives: 42.3 us -> none  [body(): lax.psum((jnp.sum(key_weight * key_weight), jnp.sum(value_weight * value_...]
    all_gather x2 -> x0, blocking collectives: 28.4 us -> none  [the longest x1 14.2 us: body(): lax.all_gather(value_renewed.astype(jnp.bfloat16), 'fs', axis=0, tiled=True)]
    pallas_call x0 -> x2, Pallas kernels: none -> 24.2 us  [the longest x1 22.6 us: body(): pl.pallas_call(functools.partial(exchange_kernel, n, m), out_shape=(sds((...]
    psum x1 -> x0, waiting for transfers between devices: 13.8 us -> none  [body(): lax.psum(key_term.astype(jnp.bfloat16), 'fs').astype(jnp.float32)]
    dot_general x5 -> x0, matrix products: 12.1 us -> none  [the longest x1 4.96 us: body(): reduced = jnp.dot(latent, factors, preferred_element_type=jnp.float32)]
    unnamed x26 -> x22, local copies, waits for them, and re-layouts: 1.48 us -> 8.04 us
    add x2 -> x0, other arithmetic: 1.76 us -> none  [moments_and_step(): SECOND_DECAY * second + (1.0 - SECOND_DECAY) * projected * projected]
  transfers between devices with their start and end apart: 1 -> 0, of which waited for: 1 -> 0; matrix products, arithmetic and copies ran while one was open for 1% -> 0% of each run, Pallas kernels for 0% -> 0%
where the time goes in v1:
time: 33.4 us; the launch traced here: 32.9 us
  Pallas kernels  24.2 us (72%)
  local copies, waits for them, and re-layouts  8.04 us (24%)
  between operations  0.71 us (2%)
    pallas_call x1, Pallas kernels, body(): pl.pallas_call(functools.partial(exchange_kernel, n, m), out_shape=(sds((...  22.6 us
    unnamed x22, local copies, waits for them, and re-layouts  8.04 us
    pallas_call x1, Pallas kernels, body(): pl.pallas_call(functools.partial(update_kernel, n, float(rows * cols * n...  1.54 us

profile of v1, /device:TPU:0, one launch (start us, length us, event | category | flops | bytes accessed | tf_op | source)
XLA Modules:
  0.0 32.9 jit_solution(15925966920248802734)
XLA Ops:
  0.6 0.0 copy-start
  0.7 2.2 %copy-done = bf16[2048,1024]{1,0:T(8,128)(2,1)S(1)} copy-done((bf16[2048,1024]{1,0:T(8,128)(2,1)S(1)}, bf16[2048,1024]{1,0:T(8,128)(2,1)}, u32[]{:S(2)}) %copy-start) | copy-done | bytes 4194328
  2.8 0.0 copy-start.1
  2.8 1.0 %copy-done.1 = bf16[1024,256]{1,0:T(8,128)(2,1)S(1)} copy-done((bf16[1024,256]{1,0:T(8,128)(2,1)S(1)}, bf16[1024,256]{1,0:T(8,128)(2,1)}, u32[]{:S(2)}) %copy-start.1) | copy-done | bytes 524312
  3.9 0.0 copy-start.2
  3.9 1.0 %copy-done.2 = bf16[1024,256]{1,0:T(8,128)(2,1)S(1)} copy-done((bf16[1024,256]{1,0:T(8,128)(2,1)S(1)}, bf16[1024,256]{1,0:T(8,128)(2,1)}, u32[]{:S(2)}) %copy-start.2) | copy-done | bytes 524312
  4.9 0.0 copy-start.3
  4.9 1.0 %copy-done.3 = bf16[2048,128]{1,0:T(8,128)(2,1)S(1)} copy-done((bf16[2048,128]{1,0:T(8,128)(2,1)S(1)}, bf16[2048,128]{1,0:T(8,128)(2,1)}, u32[]{:S(2)}) %copy-start.3) | copy-done | bytes 524312
  6.0 0.0 copy-start.4
  6.0 1.0 %copy-done.4 = bf16[2048,128]{1,0:T(8,128)(2,1)S(1)} copy-done((bf16[2048,128]{1,0:T(8,128)(2,1)S(1)}, bf16[2048,128]{1,0:T(8,128)(2,1)}, u32[]{:S(2)}) %copy-start.4) | copy-done | bytes 524312
  7.0 0.0 copy-start.5
  7.0 0.8 %copy-done.5 = f32[128,128]{1,0:T(8,128)S(1)} copy-done((f32[128,128]{1,0:T(8,128)S(1)}, f32[128,128]{1,0:T(8,128)}, u32[]{:S(2)}) %copy-start.5) | copy-done | bytes 65560
  7.8 0.0 copy-start.6
  7.8 0.8 %copy-done.6 = f32[128,128]{1,0:T(8,128)S(1)} copy-done((f32[128,128]{1,0:T(8,128)S(1)}, f32[128,128]{1,0:T(8,128)}, u32[]{:S(2)}) %copy-start.6) | copy-done | bytes 65560
  8.7 0.0 copy-start.7
  8.7 0.0 copy-start.8
  8.7 0.0 copy-start.9
  8.7 0.0 copy-start.10
  8.7 22.6 %shard_map.186 = (bf16[8,64,128]{2,1,0:T(8,128)(2,1)S(1)}, bf16[8,2,128,128]{3,2,1,0:T(8,128)(2,1)S(1)}, f32[8,16,128]{2,1,0:T(8,128)S(1)}) custom-call(bf16[2048,1024]{1,0:T(8,128)(2,1)S(1)} %copy-done, bf16[2048,128]{1,0:T(8,128)(2,1)S(1)} %copy-done.3, bf16[2048,128]{1,0:T(8,128)(2,1)S(1)} %copy-done.4, f32[128,128]{1,0:T(8,128)S(1)} %copy-done.5, ...), custom_call_target="tpu_custom_call" | custom-call | tf_op jit(solution)/shard_map/pallas_call | solution.py:325
  31.4 0.0 copy-done.7
  31.4 0.0 copy-done.8
  31.4 0.0 copy-done.9
  31.4 0.0 copy-done.10
  31.4 1.5 %shard_map.187 = (f32[128,128]{1,0:T(8,128)}, f32[128,128]{1,0:T(8,128)}, f32[128,128]{1,0:T(8,128)}, f32[128,128]{1,0:T(8,128)}, f32[256,128]{1,0:T(8,128)}, /*...) custom-call(bf16[8,64,128]{2,1,0:T(8,128)(2,1)S(1)} %get-tuple-eleme, ...), custom_call_target="tpu_custom_call" | custom-call | tf_op jit(solution)/shard_map/pallas_call | solution.py:365
Async XLA Ops:
  0.6 2.2 %copy-start = (bf16[2048,1024]{1,0:T(8,128)(2,1)S(1)}, bf16[2048,1024]{1,0:T(8,128)(2,1)}, u32[]{:S(2)}) copy-start(bf16[2048,1024]{1,0:T(8,128)(2,1)} %latent.1) | copy-start | bytes 12582916
  2.8 1.0 %copy-start.1 = (bf16[1024,256]{1,0:T(8,128)(2,1)S(1)}, bf16[1024,256]{1,0:T(8,128)(2,1)}, u32[]{:S(2)}) copy-start(bf16[1024,256]{1,0:T(8,128)(2,1)} %refs_5_.1) | copy-start | bytes 1572868
  3.9 1.0 %copy-start.2 = (bf16[1024,256]{1,0:T(8,128)(2,1)S(1)}, bf16[1024,256]{1,0:T(8,128)(2,1)}, u32[]{:S(2)}) copy-start(bf16[1024,256]{1,0:T(8,128)(2,1)} %refs_6_.1) | copy-start | bytes 1572868
  4.9 1.0 %copy-start.3 = (bf16[2048,128]{1,0:T(8,128)(2,1)S(1)}, bf16[2048,128]{1,0:T(8,128)(2,1)}, u32[]{:S(2)}) copy-start(bf16[2048,128]{1,0:T(8,128)(2,1)} %key_cot.1) | copy-start | bytes 1572868
  6.0 1.0 %copy-start.4 = (bf16[2048,128]{1,0:T(8,128)(2,1)S(1)}, bf16[2048,128]{1,0:T(8,128)(2,1)}, u32[]{:S(2)}) copy-start(bf16[2048,128]{1,0:T(8,128)(2,1)} %value_cot.1) | copy-start | bytes 1572868
  7.0 0.8 %copy-start.5 = (f32[128,128]{1,0:T(8,128)S(1)}, f32[128,128]{1,0:T(8,128)}, u32[]{:S(2)}) copy-start(f32[128,128]{1,0:T(8,128)} %refs_3_.1) | copy-start | bytes 196612
  7.8 0.8 %copy-start.6 = (f32[128,128]{1,0:T(8,128)S(1)}, f32[128,128]{1,0:T(8,128)}, u32[]{:S(2)}) copy-start(f32[128,128]{1,0:T(8,128)} %refs_4_.1) | copy-start | bytes 196612
  8.7 22.7 %copy-start.7 = (f32[256,128]{1,0:T(8,128)S(1)}, f32[256,128]{1,0:T(8,128)}, u32[]{:S(2)}) copy-start(f32[256,128]{1,0:T(8,128)} %refs_7_.1) | copy-start | bytes 393220
  8.7 22.7 %copy-start.8 = (f32[256,128]{1,0:T(8,128)S(1)}, f32[256,128]{1,0:T(8,128)}, u32[]{:S(2)}) copy-start(f32[256,128]{1,0:T(8,128)} %refs_8_.1) | copy-start | bytes 393220
  8.7 22.7 %copy-start.9 = (f32[256,128]{1,0:T(8,128)S(1)}, f32[256,128]{1,0:T(8,128)}, u32[]{:S(2)}) copy-start(f32[256,128]{1,0:T(8,128)} %refs_9_.1) | copy-start | bytes 393220
  8.7 22.7 %copy-start.10 = (f32[256,128]{1,0:T(8,128)S(1)}, f32[256,128]{1,0:T(8,128)}, u32[]{:S(2)}) copy-start(f32[256,128]{1,0:T(8,128)} %refs_10_.1) | copy-start | bytes 393220

commit v2 on v1

--- a/solution.py
+++ b/solution.py
@@ -27,14 +27,19 @@
     value_weight,
     key_proj,
     value_proj,
+    key_first,
+    key_second,
+    value_first,
+    value_second,
     gathered,
     weights,
     squares,
+    weight_v,
+    proj_v,
+    moment_v,
     latent_v,
     cot_v,
     cot_t,
-    weight_v,
-    proj_v,
     partial,
     received,
     tp_squares,
@@ -75,6 +80,10 @@
                 (value_cot, cot_v.at[1]),
                 (key_proj, proj_v.at[0]),
                 (value_proj, proj_v.at[1]),
+                (key_first, moment_v.at[0]),
+                (key_second, moment_v.at[1]),
+                (value_first, moment_v.at[2]),
+                (value_second, moment_v.at[3]),
             )
         )
     ]
@@ -87,9 +96,11 @@
     for copy in loads[:4]:
         copy.start()
     streams[0].start()
-    for copy in loads[4:]:
+    for copy in loads[4:6]:
         copy.start()
     for copy in streams[1:]:
+        copy.start()
+    for copy in loads[6:]:
         copy.start()
 
     barrier = pltpu.get_barrier_semaphore()
@@ -124,15 +135,29 @@
             device_id_type=MESH,
         ).wait_recv()
 
+    chip = lax.div(me, 2)
+    side = lax.div(chip, (half + 1) // 2)
+
+    def far_first(k):
+        down = half - 1 - k
+        down = down - lax.div(chip - down + half, half)
+        up = k + lax.div(k - chip + half, half)
+        return down + side * (up - down)
+
+    def peers():
+        for k in range(half - 1):
+            base = 2 * far_first(k)
+            yield base + 1 - core
+            yield base + core
+        yield partner
+
     sent = []
     loads[0].wait()
     loads[1].wait()
     for i in range(2):
         w = weight_v[i]
         weights[me, i] = w.astype(bf16)
-        tp_squares[mine, pl.ds(8 * i, 8), :] = jnp.sum(
-            (w * w).reshape(w.shape[0] // 8, 8, w.shape[1]), axis=0
-        )
+        tp_squares[mine, pl.ds(i, 1), :] = jnp.sum(w * w, axis=0, keepdims=True)
     loads[2].wait()
     loads[3].wait()
     for i in range(2):
@@ -147,7 +172,7 @@
                 weights.at[me],
                 w_send.at[d],
                 w_recv.at[me],
-                {"fs": lax.rem(me + 2 * d, n)},
+                {"fs": 2 * far_first(d - 1) + core},
             )
         )
 
@@ -190,8 +215,7 @@
         arrived(tp_squares.at[lax.rem(mine + d, m)], t_recv.at[lax.rem(mine + d, m)])
     squares[me] = jnp.sum(tp_squares[...], axis=0)
 
-    for d in range(n - 1, 0, -1):
-        peer = lax.rem(me + d, n)
+    for d, peer in enumerate(peers()):
         sent.append(
             send(
                 partial.at[pl.ds(peer * piece, piece)],
@@ -216,14 +240,14 @@
         peer = lax.rem(me + d, n)
         arrived(received.at[peer], rs_recv.at[peer])
     gathered[me] = jnp.sum(received[...].astype(f32), axis=0).astype(bf16)
-    for d in range(n - 1, 0, -1):
+    for d, peer in enumerate(peers()):
         sent.append(
             send(
                 gathered.at[me],
                 gathered.at[me],
                 ag_send.at[d],
                 ag_recv.at[me],
-                {"fs": lax.rem(me + d, n)},
+                {"fs": peer},
             )
         )
     for d in range(1, half):
@@ -247,56 +271,55 @@
     for d in range(1, n):
         peer = lax.rem(me + d, n)
         arrived(gathered.at[peer], ag_recv.at[peer])
+    for copy in loads[6:]:
+        copy.wait()
     for copy in sent:
         copy.wait_send()
 
 
 def update_kernel(n, entries, *refs):
-    (
-        gathered,
-        weights,
-        squares,
-        key_weight,
-        value_weight,
-        key_proj,
-        value_proj,
-        key_first,
-        key_second,
-        value_first,
-        value_second,
-    ) = refs[:11]
-    outs = refs[11:]
+    gathered, weights, squares, weight_v, proj_v, moment_v = refs[:6]
+    outs, stage, sems = refs[6:16], refs[16:26], refs[26]
     me = lax.axis_index("fs")
     f32, bf16 = jnp.float32, jnp.bfloat16
     parts = n // 2
-    tile = jnp.sum(squares[...], axis=0)
-    for i, (weight, proj, first, second) in enumerate(
-        (
-            (key_weight, key_proj, key_first, key_second),
-            (value_weight, value_proj, value_first, value_second),
-        )
-    ):
-        rows = weight.shape[0]
-        rank, cols = first.shape
+    rows, cols = weight_v.shape[1:]
+    rank = moment_v.shape[1]
+    copies = [
+        pltpu.make_async_copy(src, dst, sems.at[i])
+        for i, (src, dst) in enumerate(zip(stage, outs))
+    ]
+    normalized = []
+    for i in range(2):
         projected = (
             gathered[i * parts : (i + 1) * parts].astype(f32).reshape(rank, cols)
         )
-        first_new = FIRST_DECAY * first[...] + (1.0 - FIRST_DECAY) * projected
+        first_new = FIRST_DECAY * moment_v[2 * i] + (1.0 - FIRST_DECAY) * projected
         second_new = (
-            SECOND_DECAY * second[...] + (1.0 - SECOND_DECAY) * projected * projected
-        )
-        outs[4 + 2 * i][...] = first_new
-        outs[5 + 2 * i][...] = second_new
-        normalized = (first_new / (jnp.sqrt(second_new) + EPSILON)).astype(bf16)
-        total = jnp.sum(tile[8 * i : 8 * i + 8], keepdims=True)
+            SECOND_DECAY * moment_v[2 * i + 1]
+            + (1.0 - SECOND_DECAY) * projected * projected
+        )
+        stage[4 + 2 * i][...] = first_new
+        stage[5 + 2 * i][...] = second_new
+        copies[4 + 2 * i].start()
+        copies[5 + 2 * i].start()
+        normalized.append((first_new / (jnp.sqrt(second_new) + EPSILON)).astype(bf16))
+    tile = jnp.sum(squares[...], axis=0)
+    for i in range(2):
+        total = jnp.sum(tile[i : i + 1], keepdims=True)
         scale = LEARN_RATE * jnp.sqrt(total / entries)
-        own = proj[pl.ds(pl.multiple_of(me * rows, rows), rows), :]
-        own_step = scale * jnp.dot(own, normalized, preferred_element_type=f32)
-        outs[2 + i][...] = own_step
-        outs[i][...] = weight[...] - own_step
-        every = scale * jnp.dot(proj[...], normalized, preferred_element_type=f32)
+        every = scale * jnp.dot(proj_v[i], normalized[i], preferred_element_type=f32)
         held = weights[:, i].astype(f32).reshape(n * rows, cols)
-        outs[8 + i][...] = (held - every).astype(bf16)
+        stage[8 + i][...] = (held - every).astype(bf16)
+        copies[8 + i].start()
+        own = proj_v[i, pl.ds(pl.multiple_of(me * rows, rows), rows), :]
+        own_step = scale * jnp.dot(own, normalized[i], preferred_element_type=f32)
+        stage[2 + i][...] = own_step
+        stage[i][...] = weight_v[i] - own_step
+        copies[2 + i].start()
+        copies[i].start()
+    for copy in copies:
+        copy.wait()
 
 
 def solution(mesh):
@@ -322,25 +345,26 @@
         rank = key_proj.shape[1]
         piece = 2 * rank // n
         dma = pltpu.SemaphoreType.DMA
-        gathered, weights, squares = pl.pallas_call(
+        held = pl.pallas_call(
             functools.partial(exchange_kernel, n, m),
             out_shape=(
                 sds((n, piece, cols), bf16),
                 sds((n, 2, rows, cols), bf16),
-                sds((n, 16, cols), f32),
+                sds((n, 2, cols), f32),
+                sds((2, rows, cols), f32),
+                sds((2, width, rank), bf16),
+                sds((4, rank, cols), f32),
             ),
-            in_specs=[HBM] * 7,
-            out_specs=(VMEM,) * 3,
+            in_specs=[HBM] * 11,
+            out_specs=(VMEM,) * 6,
             scratch_shapes=[
                 pltpu.VMEM((CHUNKS, tokens, width // CHUNKS), bf16),
                 pltpu.VMEM((2, tokens, cols), bf16),
                 pltpu.VMEM((2 * cols, tokens), bf16),
-                pltpu.VMEM((2, rows, cols), f32),
-                pltpu.VMEM((2, width, rank), bf16),
                 pltpu.VMEM((2 * rank, cols), bf16),
                 pltpu.VMEM((n, piece, cols), bf16),
-                pltpu.VMEM((m, 16, cols), f32),
-                dma((6,)),
+                pltpu.VMEM((m, 2, cols), f32),
+                dma((10,)),
                 dma((CHUNKS,)),
                 dma((n,)),
                 dma((n,)),
@@ -358,29 +382,38 @@
             compiler_params=pltpu.CompilerParams(
                 collective_id=0, has_side_effects=True, vmem_limit_bytes=24 << 20
             ),
-        )(latent, key_cot, value_cot, key_weight, value_weight, key_proj, value_proj)
+        )(
+            *(
+                pltpu.with_memory_space_constraint(x, pltpu.MemorySpace.HBM)
+                for x in (
+                    latent,
+                    key_cot,
+                    value_cot,
+                    key_weight,
+                    value_weight,
+                    key_proj,
+                    value_proj,
+                    key_first,
+                    key_second,
+                    value_first,
+                    value_second,
+                )
+            )
+        )
         small = sds((rows, cols), f32)
         moment = sds((rank, cols), f32)
         copy = sds((n * rows, cols), bf16)
         return pl.pallas_call(
             functools.partial(update_kernel, n, float(rows * cols * n * m)),
             out_shape=(small,) * 4 + (moment,) * 4 + (copy,) * 2,
-            in_specs=[VMEM] * 11,
-            out_specs=(VMEM,) * 10,
+            in_specs=[VMEM] * 6,
+            out_specs=(HBM,) * 10,
+            scratch_shapes=[pltpu.VMEM((rows, cols), f32)] * 4
+            + [pltpu.VMEM((rank, cols), f32)] * 4
+            + [pltpu.VMEM((n * rows, cols), bf16)] * 2
+            + [dma((10,))],
             compiler_params=pltpu.CompilerParams(vmem_limit_bytes=24 << 20),
-        )(
-            gathered,
-            weights,
-            squares,
-            key_weight,
-            value_weight,
-            key_proj,
-            value_proj,
-            key_first,
-            key_second,
-            value_first,
-            value_second,
-        )
+        )(*held)
 
     split, column = P("fs", "tp"), P(None, "tp")
     return jax.shard_map(

time: 33.4 us -> 22.8 us (0.68)
  local copies, waits for them, and re-layouts: 8.04 us -> 0 us
  Pallas kernels: 24.2 us -> 21.9 us
    unnamed x22 -> x0, local copies, waits for them, and re-layouts: 8.04 us -> none
    pallas_call x1, Pallas kernels: 22.6 us -> 20.4 us  [body(): pl.pallas_call(functools.partial(exchange_kernel, n, m), out_shape=(sds((...]
where the time goes in v2:
time: 22.8 us; the launch traced here: 22.6 us
  Pallas kernels  21.9 us (96%)
  between operations  0.65 us (3%)
    pallas_call x1, Pallas kernels, body(): pl.pallas_call(functools.partial(exchange_kernel, n, m), out_shape=(sds((...  20.4 us
    pallas_call x1, Pallas kernels, body(): pl.pallas_call(functools.partial(update_kernel, n, float(rows * cols * n...  1.51 us

profile of v2, /device:TPU:0, one launch (start us, length us, event | category | flops | bytes accessed | tf_op | source)
XLA Modules:
  0.0 22.6 jit_solution(13489336780644520437)
XLA Ops:
  0.6 20.4 %shard_map.186 = (bf16[8,64,128]{2,1,0:T(8,128)(2,1)S(1)}, bf16[8,2,128,128]{3,2,1,0:T(8,128)(2,1)S(1)}, f32[8,2,128]{2,1,0:T(2,128)S(1)}, f32[2,128,128]{2,1,0:...) custom-call(bf16[2048,1024]{1,0:T(8,128)(2,1)} %latent.1, bf16[2048,128]{1,0:T(8,128)(2,1)} %key_cot.1, ...), custom_call_target="tpu_custom_call" | custom-call | tf_op jit(solution)/shard_map/pallas_call | solution.py:348
  21.1 1.5 %shard_map.187 = (f32[128,128]{1,0:T(8,128)}, f32[128,128]{1,0:T(8,128)}, f32[128,128]{1,0:T(8,128)}, f32[128,128]{1,0:T(8,128)}, f32[256,128]{1,0:T(8,128)}, /*...) custom-call(bf16[8,64,128]{2,1,0:T(8,128)(2,1)S(1)} %get-tuple-eleme, ...), custom_call_target="tpu_custom_call" | custom-call | tf_op jit(solution)/shard_map/pallas_call | solution.py:406
